TPU v7x, 32 devices: a whole 2x2x4 slice. The times are simulated.
32 devices in a mesh: sp: 8 (over z, y), tp: 4 (over x, core).
Axes of the slice: x: 2, y: 2, z: 4, core: 2. Of those that a mesh axis runs over, the one named last changes fastest.
Arguments:
- stream: bfloat16 [2048, 2048], P('sp', 'tp'), may hold values from -8 to 8
- norm_gain: float32 [2, 2048], P(None, 'tp'), may hold values from 0.1 to 1.9
- query_weight: bfloat16 [2, 2048, 1024], P(None, None, 'tp'), may hold values from -4 to 4
- key_weight: bfloat16 [2, 2048, 1024], P(None, None, 'tp'), may hold values from -4 to 4
- value_weight: bfloat16 [2, 2048, 1024], P(None, None, 'tp'), may hold values from -0.125 to 0.125
- out_weight: bfloat16 [2, 1024, 2048], P(None, None, 'tp'), may hold values from -1.5 to 1.5
- rel_bias: float32 [2, 16, 257], P(None, 'tp'), may hold values from -4 to 4
Outputs:
- mixed: bfloat16 [2048, 2048], P('sp', 'tp')
All inputs are finite; a program needn't handle non-finite values.
Results may differ from a plain program's by a relative error of at most 0.013.
Values may be sent and summed in bfloat16 or wider, within the bound.
A program may use at most 64 MiB of HBM per device.

v0:
```python
import jax
import jax.numpy as jnp
from jax import lax
from jax.sharding import PartitionSpec as P

D = 2048
SEG = 64
PREV = 8
CLIP = 128
LAYERS = 2
epsilon = 1e-06
masked_score = -1e30


def from_behind(shard, axis, by):
    count = lax.axis_size(axis)
    pairs = [(i, i + by) for i in range(count) if 0 <= i + by < count]
    return lax.ppermute(shard, axis, pairs)


def normalize(residual, gain):
    values_f = residual.astype(jnp.float32)
    squares = lax.psum(jnp.sum(values_f * values_f, axis=-1, keepdims=True), "tp")
    scaled = values_f * lax.rsqrt(squares / D + epsilon)
    return (scaled * gain).astype(jnp.bfloat16)


def bias_table(table, band_len):
    heads_here = table.shape[0]
    near_part = table[:, CLIP - (SEG - 1) :]
    far_count = band_len - 1 - CLIP
    far_part = jnp.broadcast_to(table[:, 2 * CLIP : 2 * CLIP + 1], (heads_here, far_count))
    reversed_row = jnp.concatenate([near_part, far_part], axis=1)[:, ::-1]
    slices = [
        reversed_row[:, SEG - 1 - within : SEG - 1 - within + band_len] for within in range(SEG)
    ]
    return jnp.stack(slices, axis=1)


def project_rows(rows_local, query_count, query_mat, key_mat, value_mat):
    row_count = rows_local.shape[0]
    first_query = row_count - query_count
    piece = lax.all_gather(rows_local, "tp", axis=1, tiled=True)
    query_sum = jnp.dot(piece[first_query:], query_mat, preferred_element_type=jnp.float32)
    key_sum = jnp.dot(piece, key_mat, preferred_element_type=jnp.float32)
    value_sum = jnp.dot(piece, value_mat, preferred_element_type=jnp.float32)
    return (
        query_sum.astype(jnp.bfloat16),
        key_sum.astype(jnp.bfloat16),
        value_sum.astype(jnp.bfloat16),
    )


def earlier_inputs(normed, shift_count):
    pieces = [from_behind(normed, "sp", step_back) for step_back in range(shift_count, 0, -1)]
    return jnp.concatenate(pieces, axis=0)


def band_blocks(extended, segments):
    blocked = extended.reshape((segments + PREV, SEG) + extended.shape[1:])
    return jnp.concatenate(
        [blocked[offset_seg : offset_seg + segments] for offset_seg in range(PREV + 1)], axis=1
    )


def attend(query_rows, key_ext, value_ext, position_bias, visible):
    tok_rows, head_cols = query_rows.shape
    heads_here = position_bias.shape[0]
    head_dim = head_cols // heads_here
    segments = tok_rows // SEG
    band_len = (PREV + 1) * SEG
    query_blocks = query_rows.reshape(segments, SEG, heads_here, head_dim)
    key_blocks = band_blocks(key_ext, segments).reshape(segments, band_len, heads_here, head_dim)
    value_blocks = band_blocks(value_ext, segments).reshape(
        segments, band_len, heads_here, head_dim
    )
    visible_blocks = band_blocks(visible, segments)
    scores = jnp.einsum(
        "sqhd,skhd->hsqk", query_blocks, key_blocks, preferred_element_type=jnp.float32
    )
    scores = scores * head_dim ** (-0.5) + position_bias[:, None]
    scores = jnp.where(visible_blocks[None, :, None, :], scores, masked_score)
    maximum = jnp.max(scores, axis=-1, keepdims=True)
    exponent = jnp.exp(scores - maximum)
    weights = (exponent / jnp.sum(exponent, axis=-1, keepdims=True)).astype(jnp.bfloat16)
    attended = jnp.einsum(
        "hsqk,skhd->sqhd", weights, value_blocks, preferred_element_type=jnp.float32
    )
    return attended.astype(jnp.bfloat16).reshape(tok_rows, head_cols)


def per_device(stream, norm_gain, query_weight, key_weight, value_weight, out_weight, rel_bias):
    tok_rows = stream.shape[0]
    reach_rows = PREV * SEG
    shift_count = max(1, reach_rows // tok_rows)
    band_len = reach_rows + SEG
    positions = (
        lax.axis_index("sp") * tok_rows
        - reach_rows
        + jnp.arange(reach_rows + tok_rows, dtype=jnp.int32)
    )
    visible = positions >= 0
    residual = stream
    for layer_index in range(LAYERS):
        normed = normalize(residual, norm_gain[layer_index])
        normed_ext = jnp.concatenate([earlier_inputs(normed, shift_count), normed], axis=0)
        query_rows, key_ext, value_ext = project_rows(
            normed_ext,
            tok_rows,
            query_weight[layer_index],
            key_weight[layer_index],
            value_weight[layer_index],
        )
        position_bias = bias_table(rel_bias[layer_index], band_len)
        attended = attend(query_rows, key_ext, value_ext, position_bias, visible)
        out_mat = out_weight[layer_index]
        summed = residual.astype(jnp.float32) + jnp.dot(
            lax.all_gather(attended, "tp", axis=1, tiled=True),
            out_mat,
            preferred_element_type=jnp.float32,
        )
        residual = summed.astype(jnp.bfloat16)
    return residual


def solution(mesh):
    placed = (
        P("sp", "tp"),
        P(None, "tp"),
        P(None, None, "tp"),
        P(None, None, "tp"),
        P(None, None, "tp"),
        P(None, None, "tp"),
        P(None, "tp", None),
    )
    return jax.shard_map(
        per_device, mesh=mesh, in_specs=placed, out_specs=P("sp", "tp"), check_vma=False
    )
```

profile of v0, /device:TPU:0, one launch (start us, length us, event | category | flops | bytes accessed | tf_op | source)
XLA Modules:
  0.0 262.6 jit_solution(17611809908315193769)
XLA Ops:
  6.5 1.1 fusion.49
  7.6 8.4 %psum.14 = f32[256,1]{0,1:T(1,128)S(1)} all-reduce(f32[256,1]{0,1:T(1,128)S(1)} %bitcast.562), channel_id=1, replica_groups=mesh['sp'=8,'tp'=4] {'tp'}, use_global_device_ids=true, to_apply=%region_1.0 | all-reduce | flops 256 | bytes 2048 | tf_op jit(solution)/shard_map/psum | solution.py:23
  16.8 1.1 fusion.51
  17.9 3.4 %collective-permute-start.1 = (bf16[256,512]{1,0:T(8,128)(2,1)S(1)}, bf16[256,512]{1,0:T(8,128)(2,1)S(1)}, u32[]{:S(2)}, u32[]{:S(2)}) collective-permute-start(bf16[256,512]{1,0:T(8,128)(2,1)S(1)} %fusion.51), channel_id=1, source_target_pairs={{0,4},{4,8},{8,12},{12,16},{16,20},{20,24},{24,28},{1,5},{5,9},{9,... | collective-permute-start | bytes 786440 | tf_op jit(solution)/shard_map/ppermute | solution.py:18
  21.3 3.5 %collective-permute-start = (bf16[256,512]{1,0:T(8,128)(2,1)S(1)}, bf16[256,512]{1,0:T(8,128)(2,1)S(1)}, u32[]{:S(2)}, u32[]{:S(2)}) collective-permute-start(bf16[256,512]{1,0:T(8,128)(2,1)S(1)} %fusion.51), channel_id=1, source_target_pairs={{0,8},{4,12},{8,16},{12,20},{16,24},{20,28},{1,9},{5,13},{9,17},{1... | collective-permute-start | bytes 786440 | tf_op jit(solution)/shard_map/ppermute | solution.py:18
  87.8 0.9 pad_maximum_fusion
  95.7 2.0 reverse.211
  98.3 6.1 %stack.454 = f32[4,64,576]{2,1,0:T(8,128)} concatenate(f32[4,1,576]{2,1,0:T(1,128)S(1)} %copy.193, f32[4,1,576]{2,1,0:T(1,128)S(1)} %copy.194, f32[4,1,576]{2,1,0:T(1,128)S(1)} %copy.195, f32[4,1,576]{2,1,0:T(1,128)S(1)} %copy.196, f32[4,1,576]{2,1,0:T(1,128)S(1)} %copy.197, f32[4,1,576]{2,1,0:T(1,128)S(1)} %copy.198, f32[4,1,576]{2,1,0:T(1,128)S(1)} %copy.199, ...), dimensions={1} | concatenate | bytes 1179648 | tf_op jit(solution)/shard_map/stack | solution.py:37
  118.5 2.1 convolution_convert_fusion.5
  121.5 2.2 convolution_convert_fusion.3
  127.8 3.1 %convolution_convert_fusion.2 = bf16[768,256]{1,0:T(8,128)(2,1)S(1)} fusion(bf16[768,2048]{1,0:T(8,128)(2,1)} %all-gather.3.cloned.1.call-done, bf16[2,2048,256]{2,1,0:T(8,128)(2,1)} %param.10), kind=kOutput, calls=%fused_computation.24 | convolution fusion | flops 805502976 | bytes 4587520 | tf_op jit(solution)/shard_map/dot_general | solution.py:45
  140.8 2.8 %concatenate.125 = bf16[4,576,4,64]{1,3,0,2:T(8,128)(2,1)S(1)} concatenate(bf16[4,64,4,64]{1,3,0,2:T(8,128)(2,1)} %copy.183, bf16[4,64,4,64]{1,3,0,2:T(8,128)(2,1)} %copy.184, bf16[4,64,4,64]{1,3,0,2:T(8,128)(2,1)} %copy.185, bf16[4,64,4,64]{1,3,0,2:T(8,128)(2,1)} %copy.186, bf16[4,64,4,64]{1,3,0,2:T(8,128)(2,1)} %copy.187, bf16[4,64,4,64]{1,3,0,2:T(8,128)(2,1)} %copy.188, ...), dimensions={1} | concatenate | bytes 2359296 | tf_op jit(solution)/shard_map/concatenate | solution.py:61
  143.6 3.7 %fusion.204 = (f32[4,4,64]{2,1,0:T(4,128)S(1)}, f32[4,4,64,576]{3,2,1,0:T(8,128)}) fusion(f32[4,64,576]{2,1,0:T(8,128)} %stack.454, pred[4,576]{1,0:T(4,128)(4,1)S(1)} %copy-done.42, bf16[4,576,4,64]{1,3,0,2:T(8,128)(2,1)S(1)} %concatenate.125, bf16[4,64,4,64]{3,2,1,0:T(4,128)(2,1)} %reshape.164), kind=kOutput, calls=%fused_computation.465 | convolution fusion | flops 78447168 | bytes 4266240 | tf_op jit(solution)/shard_map/sub | solution.py:84
  147.3 2.3 concatenate.114
  149.6 2.4 fusion.28
  152.6 6.6 %all_gather.13 = bf16[256,1024]{1,0:T(8,128)(2,1)S(1)} all-gather(bf16[256,256]{1,0:T(8,128)(2,1)S(1)} %reshape.165), channel_id=1, replica_groups=mesh['sp'=8,'tp'=4] {'tp'}, dimensions={1}, use_global_device_ids=true | all-gather | bytes 655360 | tf_op jit(solution)/shard_map/all_gather | solution.py:118
  159.5 1.8 multiply_reduce_fusion
  161.3 6.8 %psum.15 = f32[256,1]{0,1:T(1,128)S(1)} all-reduce(f32[256,1]{0,1:T(1,128)S(1)} %bitcast.563), channel_id=1, replica_groups=mesh['sp'=8,'tp'=4] {'tp'}, use_global_device_ids=true, to_apply=%region_5.6 | all-reduce | flops 256 | bytes 2048 | tf_op jit(solution)/shard_map/psum | solution.py:23
  168.2 3.4 %collective-permute-start.3 = (bf16[256,512]{1,0:T(8,128)(2,1)S(1)}, bf16[256,512]{1,0:T(8,128)(2,1)S(1)}, u32[]{:S(2)}, u32[]{:S(2)}) collective-permute-start(bf16[256,512]{1,0:T(8,128)(2,1)S(1)} %multiply_convert_fusion), channel_id=1, source_target_pairs={{0,4},{4,8},{8,12},{12,16},{16,20},{20,24},{24,28},{1,5},{5,9},{9,... | collective-permute-start | bytes 786440 | tf_op jit(solution)/shard_map/ppermute | solution.py:18
  171.7 3.5 %collective-permute-start.2 = (bf16[256,512]{1,0:T(8,128)(2,1)S(1)}, bf16[256,512]{1,0:T(8,128)(2,1)S(1)}, u32[]{:S(2)}, u32[]{:S(2)}) collective-permute-start(bf16[256,512]{1,0:T(8,128)(2,1)S(1)} %multiply_convert_fusion), channel_id=1, source_target_pairs={{0,8},{4,12},{8,16},{12,20},{16,24},{20,28},{1,9},{5,13},{9,17},{1... | collective-permute-start | bytes 786440 | tf_op jit(solution)/shard_map/ppermute | solution.py:18
  182.6 0.9 pad_maximum_fusion.1
  195.0 6.1 %stack.519 = f32[4,64,576]{2,1,0:T(8,128)} concatenate(f32[4,1,576]{2,1,0:T(1,128)S(1)} %copy.277, f32[4,1,576]{2,1,0:T(1,128)S(1)} %copy.278, f32[4,1,576]{2,1,0:T(1,128)S(1)} %copy.279, f32[4,1,576]{2,1,0:T(1,128)S(1)} %copy.280, f32[4,1,576]{2,1,0:T(1,128)S(1)} %copy.281, f32[4,1,576]{2,1,0:T(1,128)S(1)} %copy.282, f32[4,1,576]{2,1,0:T(1,128)S(1)} %copy.283, ...), dimensions={1} | concatenate | bytes 1179648 | tf_op jit(solution)/shard_map/stack | solution.py:37
  201.1 11.2 %all-gather.5.cloned.1.call-done = bf16[768,2048]{1,0:T(8,128)(2,1)} async-done(((bf16[768,512]{1,0:T(8,128)(2,1)}), bf16[768,2048]{1,0:T(8,128)(2,1)}) %all-gather.5.cloned.1.call-update) | async-done | bytes 3145744 | tf_op jit(solution)/shard_map/all_gather | solution.py:43
  212.2 2.1 convolution_convert_fusion.4
  215.3 2.2 convolution_convert_fusion.1
  221.6 3.2 %convolution_convert_fusion = bf16[768,256]{1,0:T(8,128)(2,1)S(1)} fusion(bf16[768,2048]{1,0:T(8,128)(2,1)} %all-gather.5.cloned.1.call-done, bf16[2,2048,256]{2,1,0:T(8,128)(2,1)} %param.10), kind=kOutput, calls=%fused_computation.22 | convolution fusion | flops 805502976 | bytes 4587520 | tf_op jit(solution)/shard_map/dot_general | solution.py:45
  234.6 2.8 %concatenate.147 = bf16[4,576,4,64]{1,3,0,2:T(8,128)(2,1)S(1)} concatenate(bf16[4,64,4,64]{1,3,0,2:T(8,128)(2,1)} %copy.267, bf16[4,64,4,64]{1,3,0,2:T(8,128)(2,1)} %copy.268, bf16[4,64,4,64]{1,3,0,2:T(8,128)(2,1)} %copy.269, bf16[4,64,4,64]{1,3,0,2:T(8,128)(2,1)} %copy.270, bf16[4,64,4,64]{1,3,0,2:T(8,128)(2,1)} %copy.271, bf16[4,64,4,64]{1,3,0,2:T(8,128)(2,1)} %copy.272, ...), dimensions={1} | concatenate | bytes 2359296 | tf_op jit(solution)/shard_map/concatenate | solution.py:61
  237.4 3.7 %fusion.207 = (f32[4,4,64]{2,1,0:T(4,128)S(1)}, f32[4,4,64,576]{3,2,1,0:T(8,128)}) fusion(f32[4,64,576]{2,1,0:T(8,128)} %stack.519, pred[4,576]{1,0:T(4,128)(4,1)S(1)} %copy-done.43, bf16[4,576,4,64]{1,3,0,2:T(8,128)(2,1)S(1)} %concatenate.147, bf16[4,64,4,64]{3,2,1,0:T(4,128)(2,1)} %reshape.166), kind=kOutput, calls=%fused_computation.466 | convolution fusion | flops 78447168 | bytes 4266240 | tf_op jit(solution)/shard_map/sub | solution.py:84
  241.1 2.3 concatenate.137
  243.4 2.4 fusion.25
  246.2 7.2 %all_gather.15 = bf16[256,1024]{1,0:T(8,128)(2,1)S(1)} all-gather(bf16[256,256]{1,0:T(8,128)(2,1)S(1)} %reshape.167), channel_id=1, replica_groups=mesh['sp'=8,'tp'=4] {'tp'}, dimensions={1}, use_global_device_ids=true | all-gather | bytes 655360 | tf_op jit(solution)/shard_map/all_gather | solution.py:118
  253.4 2.4 fusion.17
  (595 shorter events, 133.1 us)
Async XLA Ops:
  6.5 112.0 %all-gather.3.cloned.1.call-start = ((), (), s32[]{:S(2)}) async-start(), calls=%async_computation | async-start | bytes 3932160 | tf_op jit(solution)/shard_map/all_gather | solution.py:43
  17.9 70.0 %collective-permute-start.1 = (bf16[256,512]{1,0:T(8,128)(2,1)S(1)}, bf16[256,512]{1,0:T(8,128)(2,1)S(1)}, u32[]{:S(2)}, u32[]{:S(2)}) collective-permute-start(bf16[256,512]{1,0:T(8,128)(2,1)S(1)} %fusion.51), channel_id=1, source_target_pairs={{0,4},{4,8},{8,12},{12,16},{16,20},{20,24},{24,28},{1,5},{5,9},{9,... | collective-permute-start | bytes 786440 | tf_op jit(solution)/shard_map/ppermute | solution.py:18
  21.3 66.5 %collective-permute-start = (bf16[256,512]{1,0:T(8,128)(2,1)S(1)}, bf16[256,512]{1,0:T(8,128)(2,1)S(1)}, u32[]{:S(2)}, u32[]{:S(2)}) collective-permute-start(bf16[256,512]{1,0:T(8,128)(2,1)S(1)} %fusion.51), channel_id=1, source_target_pairs={{0,8},{4,12},{8,16},{12,20},{16,24},{20,28},{1,9},{5,13},{9,17},{1... | collective-permute-start | bytes 786440 | tf_op jit(solution)/shard_map/ppermute | solution.py:18
  88.8 123.4 %all-gather.5.cloned.1.call-start = ((), (), s32[]{:S(2)}) async-start(), calls=%async_computation.1 | async-start | bytes 3932160 | tf_op jit(solution)/shard_map/all_gather | solution.py:43
  152.5 22.7 %copy-start.27 = (f32[4,640]{1,0:T(4,128)S(1)}, f32[4,640]{1,0:T(4,128)}, u32[]{:S(2)}) copy-start(f32[4,640]{1,0:T(4,128)} %reverse.211) | copy-start | bytes 30724
  152.5 22.8 %copy-start.7 = (f32[4,1,576]{2,0,1:T(4,128)S(1)}, f32[4,1,576]{2,0,1:T(4,128)}, u32[]{:S(2)}) copy-start(f32[4,1,576]{2,0,1:T(4,128)} %slice_bitcast_fusion.8) | copy-start | bytes 27652
  152.5 22.8 %copy-start.8 = (f32[4,1,576]{2,0,1:T(4,128)S(1)}, f32[4,1,576]{2,0,1:T(4,128)}, u32[]{:S(2)}) copy-start(f32[4,1,576]{2,0,1:T(4,128)} %slice_bitcast_fusion.7) | copy-start | bytes 27652
  152.5 22.8 %copy-start.9 = (f32[4,1,576]{2,0,1:T(4,128)S(1)}, f32[4,1,576]{2,0,1:T(4,128)}, u32[]{:S(2)}) copy-start(f32[4,1,576]{2,0,1:T(4,128)} %slice_bitcast_fusion.16) | copy-start | bytes 27652
  152.5 22.8 %copy-start.10 = (f32[4,1,576]{2,0,1:T(4,128)S(1)}, f32[4,1,576]{2,0,1:T(4,128)}, u32[]{:S(2)}) copy-start(f32[4,1,576]{2,0,1:T(4,128)} %slice_bitcast_fusion.15) | copy-start | bytes 27652
  152.5 22.9 %copy-start.11 = (f32[4,1,576]{2,0,1:T(4,128)S(1)}, f32[4,1,576]{2,0,1:T(4,128)}, u32[]{:S(2)}) copy-start(f32[4,1,576]{2,0,1:T(4,128)} %slice_bitcast_fusion.14) | copy-start | bytes 27652
  152.5 22.9 %copy-start.12 = (f32[4,1,576]{2,0,1:T(4,128)S(1)}, f32[4,1,576]{2,0,1:T(4,128)}, u32[]{:S(2)}) copy-start(f32[4,1,576]{2,0,1:T(4,128)} %slice_bitcast_fusion.13) | copy-start | bytes 27652
  152.5 22.9 %copy-start.13 = (f32[4,1,576]{2,0,1:T(4,128)S(1)}, f32[4,1,576]{2,0,1:T(4,128)}, u32[]{:S(2)}) copy-start(f32[4,1,576]{2,0,1:T(4,128)} %slice_bitcast_fusion.12) | copy-start | bytes 27652
  152.5 22.9 %copy-start.14 = (f32[4,1,576]{2,0,1:T(4,128)S(1)}, f32[4,1,576]{2,0,1:T(4,128)}, u32[]{:S(2)}) copy-start(f32[4,1,576]{2,0,1:T(4,128)} %slice_bitcast_fusion.11) | copy-start | bytes 27652
  152.6 22.9 %copy-start.15 = (f32[4,1,576]{2,0,1:T(4,128)S(1)}, f32[4,1,576]{2,0,1:T(4,128)}, u32[]{:S(2)}) copy-start(f32[4,1,576]{2,0,1:T(4,128)} %slice_bitcast_fusion.10) | copy-start | bytes 27652
  152.6 23.0 %copy-start.16 = (f32[4,1,576]{2,0,1:T(4,128)S(1)}, f32[4,1,576]{2,0,1:T(4,128)}, u32[]{:S(2)}) copy-start(f32[4,1,576]{2,0,1:T(4,128)} %slice_bitcast_fusion.9) | copy-start | bytes 27652
  152.6 23.0 %copy-start.17 = (f32[4,1,576]{2,0,1:T(4,128)S(1)}, f32[4,1,576]{2,0,1:T(4,128)}, u32[]{:S(2)}) copy-start(f32[4,1,576]{2,0,1:T(4,128)} %slice_bitcast_fusion.6) | copy-start | bytes 27652
  152.6 23.0 %copy-start.18 = (f32[4,1,576]{2,0,1:T(4,128)S(1)}, f32[4,1,576]{2,0,1:T(4,128)}, u32[]{:S(2)}) copy-start(f32[4,1,576]{2,0,1:T(4,128)} %slice_bitcast_fusion.24) | copy-start | bytes 27652
  152.6 23.0 %copy-start.19 = (f32[4,1,576]{2,0,1:T(4,128)S(1)}, f32[4,1,576]{2,0,1:T(4,128)}, u32[]{:S(2)}) copy-start(f32[4,1,576]{2,0,1:T(4,128)} %slice_bitcast_fusion.23) | copy-start | bytes 27652
  152.6 23.0 %copy-start.20 = (f32[4,1,576]{2,0,1:T(4,128)S(1)}, f32[4,1,576]{2,0,1:T(4,128)}, u32[]{:S(2)}) copy-start(f32[4,1,576]{2,0,1:T(4,128)} %slice_bitcast_fusion.22) | copy-start | bytes 27652
  152.6 23.1 %copy-start.21 = (f32[4,1,576]{2,0,1:T(4,128)S(1)}, f32[4,1,576]{2,0,1:T(4,128)}, u32[]{:S(2)}) copy-start(f32[4,1,576]{2,0,1:T(4,128)} %slice_bitcast_fusion.21) | copy-start | bytes 27652
  152.6 23.1 %copy-start.22 = (f32[4,1,576]{2,0,1:T(4,128)S(1)}, f32[4,1,576]{2,0,1:T(4,128)}, u32[]{:S(2)}) copy-start(f32[4,1,576]{2,0,1:T(4,128)} %slice_bitcast_fusion.20) | copy-start | bytes 27652
  159.4 16.7 %copy-start.37 = (f32[4,1,576]{2,0,1:T(4,128)S(1)}, f32[4,1,576]{2,0,1:T(4,128)}, u32[]{:S(2)}) copy-start(f32[4,1,576]{2,0,1:T(4,128)} %slice_bitcast_fusion.40) | copy-start | bytes 27652
  159.4 16.8 %copy-start.38 = (f32[4,1,576]{2,0,1:T(4,128)S(1)}, f32[4,1,576]{2,0,1:T(4,128)}, u32[]{:S(2)}) copy-start(f32[4,1,576]{2,0,1:T(4,128)} %slice_bitcast_fusion.39) | copy-start | bytes 27652
  159.4 16.8 %copy-start.39 = (f32[4,1,576]{2,0,1:T(4,128)S(1)}, f32[4,1,576]{2,0,1:T(4,128)}, u32[]{:S(2)}) copy-start(f32[4,1,576]{2,0,1:T(4,128)} %slice_bitcast_fusion.38) | copy-start | bytes 27652
  159.4 16.8 %copy-start.40 = (f32[4,1,576]{2,0,1:T(4,128)S(1)}, f32[4,1,576]{2,0,1:T(4,128)}, u32[]{:S(2)}) copy-start(f32[4,1,576]{2,0,1:T(4,128)} %slice_bitcast_fusion.37) | copy-start | bytes 27652
  159.4 16.8 %copy-start.41 = (f32[4,1,576]{2,0,1:T(4,128)S(1)}, f32[4,1,576]{2,0,1:T(4,128)}, u32[]{:S(2)}) copy-start(f32[4,1,576]{2,0,1:T(4,128)} %slice_bitcast_fusion.36) | copy-start | bytes 27652
  159.4 21.9 %copy-start.6 = (f32[4,576]{1,0:T(4,128)S(1)}, f32[4,576]{1,0:T(4,128)}, u32[]{:S(2)}) copy-start(f32[4,576]{1,0:T(4,128)} %get-tuple-element.64) | copy-start | bytes 27652
  159.4 22.7 %copy-start.5 = (f32[4,576]{1,0:T(4,128)S(1)}, f32[4,576]{1,0:T(4,128)}, u32[]{:S(2)}) copy-start(f32[4,576]{1,0:T(4,128)} %get-tuple-element.65) | copy-start | bytes 27652
  161.3 22.8 %copy-start.1 = (f32[256,512]{1,0:T(8,128)}, f32[256,512]{1,0:T(8,128)S(1)}, u32[]{:S(2)}) copy-start(f32[256,512]{1,0:T(8,128)S(1)} %get-tuple-element.183) | copy-start | bytes 1572868
  161.3 22.3 %copy-start.4 = (f32[4,576]{1,0:T(4,128)S(1)}, f32[4,576]{1,0:T(4,128)}, u32[]{:S(2)}) copy-start(f32[4,576]{1,0:T(4,128)} %get-tuple-element.66) | copy-start | bytes 27652
  168.2 14.3 %collective-permute-start.3 = (bf16[256,512]{1,0:T(8,128)(2,1)S(1)}, bf16[256,512]{1,0:T(8,128)(2,1)S(1)}, u32[]{:S(2)}, u32[]{:S(2)}) collective-permute-start(bf16[256,512]{1,0:T(8,128)(2,1)S(1)} %multiply_convert_fusion), channel_id=1, source_target_pairs={{0,4},{4,8},{8,12},{12,16},{16,20},{20,24},{24,28},{1,5},{5,9},{9,... | collective-permute-start | bytes 786440 | tf_op jit(solution)/shard_map/ppermute | solution.py:18
  171.7 10.9 %collective-permute-start.2 = (bf16[256,512]{1,0:T(8,128)(2,1)S(1)}, bf16[256,512]{1,0:T(8,128)(2,1)S(1)}, u32[]{:S(2)}, u32[]{:S(2)}) collective-permute-start(bf16[256,512]{1,0:T(8,128)(2,1)S(1)} %multiply_convert_fusion), channel_id=1, source_target_pairs={{0,8},{4,12},{8,16},{12,20},{16,24},{20,28},{1,9},{5,13},{9,17},{1... | collective-permute-start | bytes 786440 | tf_op jit(solution)/shard_map/ppermute | solution.py:18
  (20 other events, 265.0 us)
Sparse Core Ops, SparseCore 0:
  88.9 27.0 all-gather.2
  183.7 28.5 all-gather.4
where the time goes:
time: 264 us; the launch traced here: 263 us
  local copies, waits for them, and re-layouts  155 us (59%)
  matrix products  31.4 us (12%)
  blocking collectives  29 us (11%)
  between operations  15.7 us (6%)
  starting transfers between devices  14.1 us (5%)
  waiting for transfers between devices  11.2 us (4%)
  other arithmetic  6.69 us (3%)
    unnamed x222, local copies, waits for them, and re-layouts  59.2 us
    another operation x256, local copies, waits for them, and re-layouts, bias_table(): return jnp.stack(slices, axis=1)  52.5 us
    concatenate x77, local copies, waits for them, and re-layouts, band_blocks(): jnp.concatenate([blocked[offset_seg:offset_seg + segments] for offset_seg...  37.9 us
    psum x2, blocking collectives, normalize(): lax.psum(jnp.sum(values_f * values_f, axis=-1, keepdims=True), 'tp')  15.2 us
    ppermute x4, starting transfers between devices, from_behind(): return lax.ppermute(shard, axis, pairs)  13.8 us
    all_gather x2, blocking collectives, per_device(): lax.all_gather(attended, 'tp', axis=1, tiled=True)  13.8 us
    all_gather x2, waiting for transfers between devices, project_rows(): piece = lax.all_gather(rows_local, 'tp', axis=1, tiled=True)  11.2 us
    sub x2, matrix products, attend(): exponent = jnp.exp(scores - maximum)  7.36 us
  transfers between devices with their start and end apart: 6, of which 1 were waited for; matrix products, arithmetic and copies ran while one was open for 44% of the time, Pallas kernels for 0%

commit v1 on v0

--- a/solution.py
+++ b/solution.py
@@ -10,6 +10,11 @@
 LAYERS = 2
 epsilon = 1e-06
 masked_score = -1e30
+
+
+def gathered_along(array, name, d):
+    parts = lax.all_gather(array, name)
+    return jnp.concatenate(parts, axis=d)
 
 
 def from_behind(shard, axis, by):
@@ -115,9 +120,7 @@
         attended = attend(query_rows, key_ext, value_ext, position_bias, visible)
         out_mat = out_weight[layer_index]
         summed = residual.astype(jnp.float32) + jnp.dot(
-            lax.all_gather(attended, "tp", axis=1, tiled=True),
-            out_mat,
-            preferred_element_type=jnp.float32,
+            gathered_along(attended, "tp", 1), out_mat, preferred_element_type=jnp.float32
         )
         residual = summed.astype(jnp.bfloat16)
     return residual

time: 264 us -> 264 us (level)
  no operation moved by 1% of the time
where the time goes in v1:
time: 264 us; the launch traced here: 263 us
  local copies, waits for them, and re-layouts  155 us (59%)
  matrix products  31.2 us (12%)
  blocking collectives  28.9 us (11%)
  between operations  15.8 us (6%)
  starting transfers between devices  14.1 us (5%)
  waiting for transfers between devices  11.2 us (4%)
  other arithmetic  6.69 us (3%)
    unnamed x222, local copies, waits for them, and re-layouts  59.2 us
    another operation x256, local copies, waits for them, and re-layouts, bias_table(): return jnp.stack(slices, axis=1)  52.5 us
    concatenate x77, local copies, waits for them, and re-layouts, band_blocks(): jnp.concatenate([blocked[offset_seg:offset_seg + segments] for offset_seg...  37.9 us
    psum x2, blocking collectives, normalize(): lax.psum(jnp.sum(values_f * values_f, axis=-1, keepdims=True), 'tp')  15.2 us
    ppermute x4, starting transfers between devices, from_behind(): return lax.ppermute(shard, axis, pairs)  13.8 us
    all_gather x2, blocking collectives, gathered_along(): parts = lax.all_gather(array, name)  13.7 us
    all_gather x2, waiting for transfers between devices, project_rows(): piece = lax.all_gather(rows_local, 'tp', axis=1, tiled=True)  11.2 us
    sub x2, matrix products, attend(): exponent = jnp.exp(scores - maximum)  7.35 us
  transfers between devices with their start and end apart: 6, of which 1 were waited for; matrix products, arithmetic and copies ran while one was open for 44% of the time, Pallas kernels for 0%

profile of v1, /device:TPU:0, one launch (start us, length us, event | category | flops | bytes accessed | tf_op | source)
XLA Modules:
  0.0 262.8 jit_solution(10276899425010949764)
XLA Ops:
  6.5 1.1 fusion.49
  7.6 8.4 %psum.14 = f32[256,1]{0,1:T(1,128)S(1)} all-reduce(f32[256,1]{0,1:T(1,128)S(1)} %bitcast.570), channel_id=1, replica_groups=mesh['sp'=8,'tp'=4] {'tp'}, use_global_device_ids=true, to_apply=%region_1.0 | all-reduce | flops 256 | bytes 2048 | tf_op jit(solution)/shard_map/psum | solution.py:28
  16.8 1.1 fusion.51
  17.9 3.4 %collective-permute-start.1 = (bf16[256,512]{1,0:T(8,128)(2,1)S(1)}, bf16[256,512]{1,0:T(8,128)(2,1)S(1)}, u32[]{:S(2)}, u32[]{:S(2)}) collective-permute-start(bf16[256,512]{1,0:T(8,128)(2,1)S(1)} %fusion.51), channel_id=1, source_target_pairs={{0,4},{4,8},{8,12},{12,16},{16,20},{20,24},{24,28},{1,5},{5,9},{9,... | collective-permute-start | bytes 786440 | tf_op jit(solution)/shard_map/ppermute | solution.py:23
  21.3 3.5 %collective-permute-start = (bf16[256,512]{1,0:T(8,128)(2,1)S(1)}, bf16[256,512]{1,0:T(8,128)(2,1)S(1)}, u32[]{:S(2)}, u32[]{:S(2)}) collective-permute-start(bf16[256,512]{1,0:T(8,128)(2,1)S(1)} %fusion.51), channel_id=1, source_target_pairs={{0,8},{4,12},{8,16},{12,20},{16,24},{20,28},{1,9},{5,13},{9,17},{1... | collective-permute-start | bytes 786440 | tf_op jit(solution)/shard_map/ppermute | solution.py:23
  87.8 0.9 pad_maximum_fusion
  95.7 2.0 reverse.211
  98.3 6.1 %stack.454 = f32[4,64,576]{2,1,0:T(8,128)} concatenate(f32[4,1,576]{2,1,0:T(1,128)S(1)} %copy.363, f32[4,1,576]{2,1,0:T(1,128)S(1)} %copy.364, f32[4,1,576]{2,1,0:T(1,128)S(1)} %copy.365, f32[4,1,576]{2,1,0:T(1,128)S(1)} %copy.366, f32[4,1,576]{2,1,0:T(1,128)S(1)} %copy.367, f32[4,1,576]{2,1,0:T(1,128)S(1)} %copy.368, f32[4,1,576]{2,1,0:T(1,128)S(1)} %copy.369, ...), dimensions={1} | concatenate | bytes 1179648 | tf_op jit(solution)/shard_map/stack | solution.py:42
  118.5 2.1 convolution_convert_fusion.5
  121.5 2.2 convolution_convert_fusion.3
  127.8 3.1 %convolution_convert_fusion.2 = bf16[768,256]{1,0:T(8,128)(2,1)S(1)} fusion(bf16[768,2048]{1,0:T(8,128)(2,1)} %all-gather.3.cloned.1.call-done, bf16[2,2048,256]{2,1,0:T(8,128)(2,1)} %param.10), kind=kOutput, calls=%fused_computation.24 | convolution fusion | flops 805502976 | bytes 4587520 | tf_op jit(solution)/shard_map/dot_general | solution.py:50
  140.8 2.8 %concatenate.125 = bf16[4,576,4,64]{1,3,0,2:T(8,128)(2,1)S(1)} concatenate(bf16[4,64,4,64]{1,3,0,2:T(8,128)(2,1)} %copy.353, bf16[4,64,4,64]{1,3,0,2:T(8,128)(2,1)} %copy.354, bf16[4,64,4,64]{1,3,0,2:T(8,128)(2,1)} %copy.355, bf16[4,64,4,64]{1,3,0,2:T(8,128)(2,1)} %copy.356, bf16[4,64,4,64]{1,3,0,2:T(8,128)(2,1)} %copy.357, bf16[4,64,4,64]{1,3,0,2:T(8,128)(2,1)} %copy.358, ...), dimensions={1} | concatenate | bytes 2359296 | tf_op jit(solution)/shard_map/concatenate | solution.py:66
  143.6 3.7 %fusion.204 = (f32[4,4,64]{2,1,0:T(4,128)S(1)}, f32[4,4,64,576]{3,2,1,0:T(8,128)}) fusion(f32[4,64,576]{2,1,0:T(8,128)} %stack.454, pred[4,576]{1,0:T(4,128)(4,1)S(1)} %copy-done.42, bf16[4,576,4,64]{1,3,0,2:T(8,128)(2,1)S(1)} %concatenate.125, bf16[4,64,4,64]{3,2,1,0:T(4,128)(2,1)} %reshape.170), kind=kOutput, calls=%fused_computation.465 | convolution fusion | flops 78447168 | bytes 4266240 | tf_op jit(solution)/shard_map/sub | solution.py:89
  147.3 2.3 concatenate.114
  149.6 2.4 fusion.28
  152.4 6.5 %all_gather.13 = bf16[4,256,256]{2,1,0:T(8,128)(2,1)S(1)} all-gather(bf16[1,256,256]{2,1,0:T(8,128)(2,1)S(1)} %all_gather_reshape.6), channel_id=1, replica_groups=mesh['sp'=8,'tp'=4] {'tp'}, dimensions={0}, use_global_device_ids=true | all-gather | bytes 655360 | tf_op jit(solution)/shard_map/all_gather | solution.py:16
  159.5 1.8 multiply_reduce_fusion
  161.3 6.8 %psum.15 = f32[256,1]{0,1:T(1,128)S(1)} all-reduce(f32[256,1]{0,1:T(1,128)S(1)} %bitcast.571), channel_id=1, replica_groups=mesh['sp'=8,'tp'=4] {'tp'}, use_global_device_ids=true, to_apply=%region_5.6 | all-reduce | flops 256 | bytes 2048 | tf_op jit(solution)/shard_map/psum | solution.py:28
  168.3 3.4 %collective-permute-start.3 = (bf16[256,512]{1,0:T(8,128)(2,1)S(1)}, bf16[256,512]{1,0:T(8,128)(2,1)S(1)}, u32[]{:S(2)}, u32[]{:S(2)}) collective-permute-start(bf16[256,512]{1,0:T(8,128)(2,1)S(1)} %multiply_convert_fusion), channel_id=1, source_target_pairs={{0,4},{4,8},{8,12},{12,16},{16,20},{20,24},{24,28},{1,5},{5,9},{9,... | collective-permute-start | bytes 786440 | tf_op jit(solution)/shard_map/ppermute | solution.py:23
  171.7 3.5 %collective-permute-start.2 = (bf16[256,512]{1,0:T(8,128)(2,1)S(1)}, bf16[256,512]{1,0:T(8,128)(2,1)S(1)}, u32[]{:S(2)}, u32[]{:S(2)}) collective-permute-start(bf16[256,512]{1,0:T(8,128)(2,1)S(1)} %multiply_convert_fusion), channel_id=1, source_target_pairs={{0,8},{4,12},{8,16},{12,20},{16,24},{20,28},{1,9},{5,13},{9,17},{1... | collective-permute-start | bytes 786440 | tf_op jit(solution)/shard_map/ppermute | solution.py:23
  182.6 0.9 pad_maximum_fusion.1
  195.0 6.1 %stack.519 = f32[4,64,576]{2,1,0:T(8,128)} concatenate(f32[4,1,576]{2,1,0:T(1,128)S(1)} %copy.448, f32[4,1,576]{2,1,0:T(1,128)S(1)} %copy.449, f32[4,1,576]{2,1,0:T(1,128)S(1)} %copy.450, f32[4,1,576]{2,1,0:T(1,128)S(1)} %copy.451, f32[4,1,576]{2,1,0:T(1,128)S(1)} %copy.452, f32[4,1,576]{2,1,0:T(1,128)S(1)} %copy.453, f32[4,1,576]{2,1,0:T(1,128)S(1)} %copy.454, ...), dimensions={1} | concatenate | bytes 1179648 | tf_op jit(solution)/shard_map/stack | solution.py:42
  201.1 11.2 %all-gather.5.cloned.1.call-done = bf16[768,2048]{1,0:T(8,128)(2,1)} async-done(((bf16[768,512]{1,0:T(8,128)(2,1)}), bf16[768,2048]{1,0:T(8,128)(2,1)}) %all-gather.5.cloned.1.call-update) | async-done | bytes 3145744 | tf_op jit(solution)/shard_map/all_gather | solution.py:48
  212.3 2.1 convolution_convert_fusion.4
  215.3 2.2 convolution_convert_fusion.1
  221.6 3.2 %convolution_convert_fusion = bf16[768,256]{1,0:T(8,128)(2,1)S(1)} fusion(bf16[768,2048]{1,0:T(8,128)(2,1)} %all-gather.5.cloned.1.call-done, bf16[2,2048,256]{2,1,0:T(8,128)(2,1)} %param.10), kind=kOutput, calls=%fused_computation.22 | convolution fusion | flops 805502976 | bytes 4587520 | tf_op jit(solution)/shard_map/dot_general | solution.py:50
  234.6 2.8 %concatenate.147 = bf16[4,576,4,64]{1,3,0,2:T(8,128)(2,1)S(1)} concatenate(bf16[4,64,4,64]{1,3,0,2:T(8,128)(2,1)} %copy.438, bf16[4,64,4,64]{1,3,0,2:T(8,128)(2,1)} %copy.439, bf16[4,64,4,64]{1,3,0,2:T(8,128)(2,1)} %copy.440, bf16[4,64,4,64]{1,3,0,2:T(8,128)(2,1)} %copy.441, bf16[4,64,4,64]{1,3,0,2:T(8,128)(2,1)} %copy.442, bf16[4,64,4,64]{1,3,0,2:T(8,128)(2,1)} %copy.443, ...), dimensions={1} | concatenate | bytes 2359296 | tf_op jit(solution)/shard_map/concatenate | solution.py:66
  237.4 3.7 %fusion.207 = (f32[4,4,64]{2,1,0:T(4,128)S(1)}, f32[4,4,64,576]{3,2,1,0:T(8,128)}) fusion(f32[4,64,576]{2,1,0:T(8,128)} %stack.519, pred[4,576]{1,0:T(4,128)(4,1)S(1)} %copy-done.43, bf16[4,576,4,64]{1,3,0,2:T(8,128)(2,1)S(1)} %concatenate.147, bf16[4,64,4,64]{3,2,1,0:T(4,128)(2,1)} %reshape.173), kind=kOutput, calls=%fused_computation.466 | convolution fusion | flops 78447168 | bytes 4266240 | tf_op jit(solution)/shard_map/sub | solution.py:89
  241.1 2.3 concatenate.137
  243.4 2.4 fusion.25
  246.2 7.2 %all_gather.15 = bf16[4,256,256]{2,1,0:T(8,128)(2,1)S(1)} all-gather(bf16[1,256,256]{2,1,0:T(8,128)(2,1)S(1)} %all_gather_reshape.7), channel_id=1, replica_groups=mesh['sp'=8,'tp'=4] {'tp'}, dimensions={0}, use_global_device_ids=true | all-gather | bytes 655360 | tf_op jit(solution)/shard_map/all_gather | solution.py:16
  253.6 2.4 fusion.17
  (597 shorter events, 133.5 us)
Async XLA Ops:
  6.5 112.0 %all-gather.3.cloned.1.call-start = ((), (), s32[]{:S(2)}) async-start(), calls=%async_computation | async-start | bytes 3932160 | tf_op jit(solution)/shard_map/all_gather | solution.py:48
  17.9 70.0 %collective-permute-start.1 = (bf16[256,512]{1,0:T(8,128)(2,1)S(1)}, bf16[256,512]{1,0:T(8,128)(2,1)S(1)}, u32[]{:S(2)}, u32[]{:S(2)}) collective-permute-start(bf16[256,512]{1,0:T(8,128)(2,1)S(1)} %fusion.51), channel_id=1, source_target_pairs={{0,4},{4,8},{8,12},{12,16},{16,20},{20,24},{24,28},{1,5},{5,9},{9,... | collective-permute-start | bytes 786440 | tf_op jit(solution)/shard_map/ppermute | solution.py:23
  21.3 66.5 %collective-permute-start = (bf16[256,512]{1,0:T(8,128)(2,1)S(1)}, bf16[256,512]{1,0:T(8,128)(2,1)S(1)}, u32[]{:S(2)}, u32[]{:S(2)}) collective-permute-start(bf16[256,512]{1,0:T(8,128)(2,1)S(1)} %fusion.51), channel_id=1, source_target_pairs={{0,8},{4,12},{8,16},{12,20},{16,24},{20,28},{1,9},{5,13},{9,17},{1... | collective-permute-start | bytes 786440 | tf_op jit(solution)/shard_map/ppermute | solution.py:23
  88.8 123.5 %all-gather.5.cloned.1.call-start = ((), (), s32[]{:S(2)}) async-start(), calls=%async_computation.1 | async-start | bytes 3932160 | tf_op jit(solution)/shard_map/all_gather | solution.py:48
  159.3 16.4 %copy-start.19 = (f32[4,1,576]{2,0,1:T(4,128)S(1)}, f32[4,1,576]{2,0,1:T(4,128)}, u32[]{:S(2)}) copy-start(f32[4,1,576]{2,0,1:T(4,128)} %slice_bitcast_fusion.23) | copy-start | bytes 27652
  159.3 16.4 %copy-start.20 = (f32[4,1,576]{2,0,1:T(4,128)S(1)}, f32[4,1,576]{2,0,1:T(4,128)}, u32[]{:S(2)}) copy-start(f32[4,1,576]{2,0,1:T(4,128)} %slice_bitcast_fusion.22) | copy-start | bytes 27652
  159.3 16.4 %copy-start.21 = (f32[4,1,576]{2,0,1:T(4,128)S(1)}, f32[4,1,576]{2,0,1:T(4,128)}, u32[]{:S(2)}) copy-start(f32[4,1,576]{2,0,1:T(4,128)} %slice_bitcast_fusion.21) | copy-start | bytes 27652
  159.3 16.4 %copy-start.22 = (f32[4,1,576]{2,0,1:T(4,128)S(1)}, f32[4,1,576]{2,0,1:T(4,128)}, u32[]{:S(2)}) copy-start(f32[4,1,576]{2,0,1:T(4,128)} %slice_bitcast_fusion.20) | copy-start | bytes 27652
  159.3 16.5 %copy-start.23 = (f32[4,1,576]{2,0,1:T(4,128)S(1)}, f32[4,1,576]{2,0,1:T(4,128)}, u32[]{:S(2)}) copy-start(f32[4,1,576]{2,0,1:T(4,128)} %slice_bitcast_fusion.19) | copy-start | bytes 27652
  159.3 16.5 %copy-start.24 = (f32[4,1,576]{2,0,1:T(4,128)S(1)}, f32[4,1,576]{2,0,1:T(4,128)}, u32[]{:S(2)}) copy-start(f32[4,1,576]{2,0,1:T(4,128)} %slice_bitcast_fusion.18) | copy-start | bytes 27652
  159.3 16.5 %copy-start.25 = (f32[4,1,576]{2,0,1:T(4,128)S(1)}, f32[4,1,576]{2,0,1:T(4,128)}, u32[]{:S(2)}) copy-start(f32[4,1,576]{2,0,1:T(4,128)} %slice_bitcast_fusion.17) | copy-start | bytes 27652
  159.3 16.5 %copy-start.26 = (f32[4,1,576]{2,0,1:T(4,128)S(1)}, f32[4,1,576]{2,0,1:T(4,128)}, u32[]{:S(2)}) copy-start(f32[4,1,576]{2,0,1:T(4,128)} %slice_bitcast_fusion.5) | copy-start | bytes 27652
  159.4 16.5 %copy-start.28 = (f32[4,1,576]{2,0,1:T(4,128)S(1)}, f32[4,1,576]{2,0,1:T(4,128)}, u32[]{:S(2)}) copy-start(f32[4,1,576]{2,0,1:T(4,128)} %slice_bitcast_fusion.32) | copy-start | bytes 27652
  159.4 16.5 %copy-start.29 = (f32[4,1,576]{2,0,1:T(4,128)S(1)}, f32[4,1,576]{2,0,1:T(4,128)}, u32[]{:S(2)}) copy-start(f32[4,1,576]{2,0,1:T(4,128)} %slice_bitcast_fusion.31) | copy-start | bytes 27652
  159.4 16.6 %copy-start.30 = (f32[4,1,576]{2,0,1:T(4,128)S(1)}, f32[4,1,576]{2,0,1:T(4,128)}, u32[]{:S(2)}) copy-start(f32[4,1,576]{2,0,1:T(4,128)} %slice_bitcast_fusion.30) | copy-start | bytes 27652
  159.4 16.6 %copy-start.31 = (f32[4,1,576]{2,0,1:T(4,128)S(1)}, f32[4,1,576]{2,0,1:T(4,128)}, u32[]{:S(2)}) copy-start(f32[4,1,576]{2,0,1:T(4,128)} %slice_bitcast_fusion.29) | copy-start | bytes 27652
  159.4 16.6 %copy-start.32 = (f32[4,1,576]{2,0,1:T(4,128)S(1)}, f32[4,1,576]{2,0,1:T(4,128)}, u32[]{:S(2)}) copy-start(f32[4,1,576]{2,0,1:T(4,128)} %slice_bitcast_fusion.28) | copy-start | bytes 27652
  159.4 16.6 %copy-start.33 = (f32[4,1,576]{2,0,1:T(4,128)S(1)}, f32[4,1,576]{2,0,1:T(4,128)}, u32[]{:S(2)}) copy-start(f32[4,1,576]{2,0,1:T(4,128)} %slice_bitcast_fusion.27) | copy-start | bytes 27652
  159.4 16.6 %copy-start.34 = (f32[4,1,576]{2,0,1:T(4,128)S(1)}, f32[4,1,576]{2,0,1:T(4,128)}, u32[]{:S(2)}) copy-start(f32[4,1,576]{2,0,1:T(4,128)} %slice_bitcast_fusion.26) | copy-start | bytes 27652
  159.4 16.7 %copy-start.35 = (f32[4,1,576]{2,0,1:T(4,128)S(1)}, f32[4,1,576]{2,0,1:T(4,128)}, u32[]{:S(2)}) copy-start(f32[4,1,576]{2,0,1:T(4,128)} %slice_bitcast_fusion.25) | copy-start | bytes 27652
  159.4 16.7 %copy-start.36 = (f32[4,1,576]{2,0,1:T(4,128)S(1)}, f32[4,1,576]{2,0,1:T(4,128)}, u32[]{:S(2)}) copy-start(f32[4,1,576]{2,0,1:T(4,128)} %slice_bitcast_fusion.4) | copy-start | bytes 27652
  159.4 16.7 %copy-start.37 = (f32[4,1,576]{2,0,1:T(4,128)S(1)}, f32[4,1,576]{2,0,1:T(4,128)}, u32[]{:S(2)}) copy-start(f32[4,1,576]{2,0,1:T(4,128)} %slice_bitcast_fusion.40) | copy-start | bytes 27652
  159.5 16.7 %copy-start.38 = (f32[4,1,576]{2,0,1:T(4,128)S(1)}, f32[4,1,576]{2,0,1:T(4,128)}, u32[]{:S(2)}) copy-start(f32[4,1,576]{2,0,1:T(4,128)} %slice_bitcast_fusion.39) | copy-start | bytes 27652
  159.5 16.7 %copy-start.39 = (f32[4,1,576]{2,0,1:T(4,128)S(1)}, f32[4,1,576]{2,0,1:T(4,128)}, u32[]{:S(2)}) copy-start(f32[4,1,576]{2,0,1:T(4,128)} %slice_bitcast_fusion.38) | copy-start | bytes 27652
  159.5 16.8 %copy-start.40 = (f32[4,1,576]{2,0,1:T(4,128)S(1)}, f32[4,1,576]{2,0,1:T(4,128)}, u32[]{:S(2)}) copy-start(f32[4,1,576]{2,0,1:T(4,128)} %slice_bitcast_fusion.37) | copy-start | bytes 27652
  159.5 16.8 %copy-start.41 = (f32[4,1,576]{2,0,1:T(4,128)S(1)}, f32[4,1,576]{2,0,1:T(4,128)}, u32[]{:S(2)}) copy-start(f32[4,1,576]{2,0,1:T(4,128)} %slice_bitcast_fusion.36) | copy-start | bytes 27652
  159.5 21.8 %copy-start.6 = (f32[4,576]{1,0:T(4,128)S(1)}, f32[4,576]{1,0:T(4,128)}, u32[]{:S(2)}) copy-start(f32[4,576]{1,0:T(4,128)} %get-tuple-element.64) | copy-start | bytes 27652
  159.5 22.6 %copy-start.5 = (f32[4,576]{1,0:T(4,128)S(1)}, f32[4,576]{1,0:T(4,128)}, u32[]{:S(2)}) copy-start(f32[4,576]{1,0:T(4,128)} %get-tuple-element.65) | copy-start | bytes 27652
  161.3 22.8 %copy-start.1 = (f32[256,512]{1,0:T(8,128)}, f32[256,512]{1,0:T(8,128)S(1)}, u32[]{:S(2)}) copy-start(f32[256,512]{1,0:T(8,128)S(1)} %get-tuple-element.183) | copy-start | bytes 1572868
  161.3 22.3 %copy-start.4 = (f32[4,576]{1,0:T(4,128)S(1)}, f32[4,576]{1,0:T(4,128)}, u32[]{:S(2)}) copy-start(f32[4,576]{1,0:T(4,128)} %get-tuple-element.66) | copy-start | bytes 27652
  168.3 14.3 %collective-permute-start.3 = (bf16[256,512]{1,0:T(8,128)(2,1)S(1)}, bf16[256,512]{1,0:T(8,128)(2,1)S(1)}, u32[]{:S(2)}, u32[]{:S(2)}) collective-permute-start(bf16[256,512]{1,0:T(8,128)(2,1)S(1)} %multiply_convert_fusion), channel_id=1, source_target_pairs={{0,4},{4,8},{8,12},{12,16},{16,20},{20,24},{24,28},{1,5},{5,9},{9,... | collective-permute-start | bytes 786440 | tf_op jit(solution)/shard_map/ppermute | solution.py:23
  171.7 10.9 %collective-permute-start.2 = (bf16[256,512]{1,0:T(8,128)(2,1)S(1)}, bf16[256,512]{1,0:T(8,128)(2,1)S(1)}, u32[]{:S(2)}, u32[]{:S(2)}) collective-permute-start(bf16[256,512]{1,0:T(8,128)(2,1)S(1)} %multiply_convert_fusion), channel_id=1, source_target_pairs={{0,8},{4,12},{8,16},{12,20},{16,24},{20,28},{1,9},{5,13},{9,17},{1... | collective-permute-start | bytes 786440 | tf_op jit(solution)/shard_map/ppermute | solution.py:23
  (20 other events, 255.8 us)
Sparse Core Ops, SparseCore 0:
  88.9 27.0 all-gather.2
  183.7 28.5 all-gather.4
